TPU v7x, 32 devices: a whole 2x2x4 slice. The times are simulated.
32 devices in a mesh: sp: 8 (over z, x), tp: 4 (over y, core).
Axes of the slice: x: 2, y: 2, z: 4, core: 2. Of those that a mesh axis runs over, the one named last changes fastest.
Arguments:
- tokens: bfloat16 [8, 768, 2048], P('sp', 'tp'), may hold values from -100 to 100
- norm_gain: float32 [2048], replicated, may hold values from 0.1 to 1.9
- key_weight: bfloat16 [2048, 1024], P('sp', 'tp'), may hold values from -0.125 to 0.125
- value_weight: bfloat16 [2048, 1024], P('sp', 'tp'), may hold values from -0.125 to 0.125
- cum_gate: float32 [8, 32, 768], P('sp', None, 'tp'), may hold values from -119 to 0, as said below
- new_gate: float32 [8, 32], P('sp', 'tp'), may hold values from -119 to 0
- new_query: bfloat16 [8, 2048], P('sp', 'tp'), may hold values from -128 to 128
- new_kv: bfloat16 [8, 16, 128], P('sp', 'tp'), may hold values from -4 to 4
Outputs:
- kv_cache: bfloat16 [8, 16, 768, 128], P('sp', 'tp')
- gate_log_cache: float32 [8, 32, 768], P('sp', 'tp')
- read_out: bfloat16 [8, 2048], P('sp', 'tp')
Inputs may be any that keep to these rules, and one draw needn't show every extreme that they name: Along positions cum_gate never rises; new_gate is at most the last position's value of its prompt and head.
All inputs are finite; a program needn't handle non-finite values.
Results may differ from a plain program's by a relative error of at most 0.0071.
Values may be sent and summed in bfloat16 or wider, within the bound.
A program may use at most 64 MiB of HBM per device.

v0:
```python
import math

import jax
import jax.numpy as jnp
from jax import lax
from jax.sharding import PartitionSpec as P

HEAD = 64


def normalize(rows, norm_gain):
    widened = rows.astype(jnp.float32)
    inv_rms = lax.rsqrt(jnp.mean(widened * widened, axis=-1, keepdims=True) + 1e-06)
    scaled = (widened * norm_gain).astype(jnp.bfloat16)
    return (scaled, inv_rms)


def per_device(tokens, norm_gain, key_weight, value_weight, cum_gate, new_gate, new_query, new_kv):
    key_rows, value_rows = (
        lax.all_gather(key_weight, "sp", axis=0, tiled=True),
        lax.all_gather(value_weight, "sp", axis=0, tiled=True),
    )
    prompts, positions, model_width = tokens.shape
    local_width = key_rows.shape[1]
    kv_here = local_width // HEAD
    gate_here = lax.all_to_all(cum_gate, "tp", split_axis=1, concat_axis=2, tiled=True)
    both_weights = jnp.concatenate([key_rows, value_rows], axis=1)
    piece = lax.all_gather(tokens, "tp", axis=1, tiled=True)
    scaled, inv_rms = normalize(piece, norm_gain)
    flat = scaled.reshape(-1, model_width)
    product = jnp.dot(flat, both_weights, preferred_element_type=jnp.float32)
    product = product.reshape(piece.shape[0], piece.shape[1], 2 * local_width) * inv_rms
    projected = product.astype(jnp.bfloat16)
    length = projected.shape[1]
    key_heads = projected[:, :, :local_width].reshape(prompts, length, kv_here, HEAD)
    value_heads = projected[:, :, local_width:].reshape(prompts, length, kv_here, HEAD)
    cache_local_copy = jnp.transpose(
        jnp.concatenate([key_heads, value_heads], axis=3), (0, 2, 1, 3)
    )
    length = cache_local_copy.shape[2]
    heads_here = gate_here.shape[1]
    group = heads_here // kv_here
    scale_factor = 1.0 / math.sqrt(HEAD)
    keys = cache_local_copy[..., :HEAD]
    values = cache_local_copy[..., HEAD:]
    query = new_query.reshape(prompts, kv_here, group, HEAD)
    own_key = new_kv[..., :HEAD].astype(jnp.float32)
    own_value = new_kv[..., HEAD:].astype(jnp.float32)
    score = (
        jnp.einsum("skgd,sktd->skgt", query, keys, preferred_element_type=jnp.float32)
        * scale_factor
    )
    score = (
        score
        + new_gate.reshape(prompts, kv_here, group)[..., None]
        - gate_here.reshape(prompts, kv_here, group, length)
    )
    own = jnp.sum(query.astype(jnp.float32) * own_key[:, :, None, :], axis=3) * scale_factor
    top = jnp.maximum(jnp.max(score, axis=3), own)
    expo = jnp.exp(score - top[..., None])
    own_factor = jnp.exp(own - top)
    total = jnp.sum(expo, axis=3) + own_factor
    weights = expo.astype(jnp.bfloat16)
    numer = jnp.einsum("skgt,sktd->skgd", weights, values, preferred_element_type=jnp.float32)
    numer = numer + own_factor[..., None] * own_value[:, :, None, :]
    read_out = (numer / total[..., None]).reshape(prompts, heads_here * HEAD).astype(jnp.bfloat16)
    return (cache_local_copy, gate_here, read_out)


def solution(mesh):
    in_specs = (
        P("sp", "tp", None),
        P(),
        P("sp", "tp"),
        P("sp", "tp"),
        P("sp", None, "tp"),
        P("sp", "tp"),
        P("sp", "tp"),
        P("sp", "tp", None),
    )
    out_specs = (P("sp", "tp", None, None), P("sp", "tp", None), P("sp", "tp"))
    return jax.shard_map(
        per_device, mesh=mesh, in_specs=in_specs, out_specs=out_specs, check_vma=False
    )
```

profile of v0, /device:TPU:0, one launch (start us, length us, event | category | flops | bytes accessed | tf_op | source)
XLA Modules:
  0.0 137.1 jit_solution(10675789589863301267)
XLA Ops:
  7.2 0.0 all-gather.4.cloned.1.call-start
  7.2 0.7 all-gather.4.cloned.1.call-update
  7.9 0.0 all-gather.6.cloned.1.call-start
  8.0 0.7 all-gather.6.cloned.1.call-update
  8.7 0.0 all-gather.8.cloned.1.call-start
  8.7 0.7 all-gather.8.cloned.1.call-update
  9.4 1.4 %copy.15 = f32[1,32,192]{2,0,1:T(1,128)} copy(f32[1,32,192]{2,1,0:T(8,128)} %param.12) | data formatting | bytes 49152 | tf_op args[4]
  10.8 4.3 %all-to-all-start = ((f32[1,32,192]{2,0,1:T(1,128)}), f32[1,32,192]{2,0,1:T(1,128)S(1)}, u32[]{:S(2)}, u32[]{:S(2)}) async-start(f32[1,32,192]{2,0,1:T(1,128)} %copy.15), calls=%async_computation | async-start | bytes 65536 | tf_op jit(solution)/shard_map/all_to_all | solution.py:26
  15.1 0.7 convert_reduce_fusion
  15.8 0.1 reshape.160
  15.8 0.8 bitcast_convert_fusion
  16.7 0.1 multiply_reduce_fusion
  16.8 0.5 broadcast.73
  17.3 1.3 reduce.14
  18.6 0.1 add.40
  18.7 0.7 reduce.6
  19.4 0.1 reshape.157
  19.5 0.0 all-to-all-done
  19.5 0.1 reshape.158
  19.6 0.7 all_to_all.16
  20.3 20.5 %all-gather.4.cloned.1.call-done = bf16[1,768,2048]{2,1,0:T(8,128)(2,1)} async-done(((bf16[1,192,2048]{2,1,0:T(8,128)(2,1)}), bf16[1,768,2048]{2,1,0:T(8,128)(2,1)}) %all-gather.4.cloned.1.call-update) | async-done | bytes 3145744 | tf_op jit(solution)/shard_map/all_gather | solution.py:28
  40.8 2.7 %fusion.1 = f32[768]{0:T(1024)S(1)} fusion(bf16[1,768,2048]{2,1,0:T(8,128)(2,1)} %all-gather.4.cloned.1.call-done), kind=kLoop, calls=%fused_computation.3 | loop fusion | flops 4717824 | bytes 3148800 | tf_op jit(solution)/shard_map/reduce_sum | solution.py:13
  43.5 39.7 %all-gather.6.cloned.1.call-done = bf16[2048,256]{1,0:T(8,128)(2,1)} async-done(((bf16[256,256]{1,0:T(8,128)(2,1)}), bf16[2048,256]{1,0:T(8,128)(2,1)}) %all-gather.6.cloned.1.call-update) | async-done | bytes 1048592 | tf_op jit(solution)/shard_map/all_gather | solution.py:20
  83.3 41.2 %all-gather.8.cloned.1.call-done = bf16[2048,256]{1,0:T(8,128)(2,1)} async-done(((bf16[256,256]{1,0:T(8,128)(2,1)}), bf16[2048,256]{1,0:T(8,128)(2,1)}) %all-gather.8.cloned.1.call-update) | async-done | bytes 1048592 | tf_op jit(solution)/shard_map/all_gather | solution.py:21
  124.4 3.5 %fusion.13 = bf16[1,768,512]{1,2,0:T(8,128)(2,1)S(1)} fusion(bf16[2048,256]{1,0:T(8,128)(2,1)} %all-gather.8.cloned.1.call-done, bf16[2048,256]{1,0:T(8,128)(2,1)} %all-gather.6.cloned.1.call-done, bf16[1,768,2048]{2,1,0:T(8,128)(2,1)S(1)} %copy-done, f32[2048]{0:T(1024)S(1)} %copy-done.1, f32[768]{0:T(1024)S(1)} %add_rsqrt_fusion), kind=kOutput, calls=%fused_computation.11 | convolution fusion | flops 1620312064 | bytes 6040576 | tf_op jit(solution)/shard_map/dot_general | solution.py:31
  127.9 0.1 fusion.29
  127.9 0.1 maximum_bitcast_fusion
  128.0 1.2 copy.17
  129.2 0.2 fusion.30
  129.4 0.2 fusion.23
  129.6 0.3 fusion.22
  129.9 0.7 convert_element_type.57
  (8 shorter events, 0.0 us)
Async XLA Ops:
  7.2 117.3 %copy-start.1 = (f32[2048]{0:T(1024)S(1)}, f32[2048]{0:T(1024)}, u32[]{:S(2)}) copy-start(f32[2048]{0:T(1024)} %param.9) | copy-start | bytes 24580
  7.2 33.6 %all-gather.4.cloned.1.call-start = ((), (), s32[]{:S(2)}) async-start(), calls=%async_computation.1 | async-start | bytes 3932160 | tf_op jit(solution)/shard_map/all_gather | solution.py:28
  7.9 75.4 %all-gather.6.cloned.1.call-start = ((), (), s32[]{:S(2)}) async-start(), calls=%async_computation.2 | async-start | bytes 1179648 | tf_op jit(solution)/shard_map/all_gather | solution.py:20
  8.7 115.8 %all-gather.8.cloned.1.call-start = ((), (), s32[]{:S(2)}) async-start(), calls=%async_computation.3 | async-start | bytes 1179648 | tf_op jit(solution)/shard_map/all_gather | solution.py:21
  10.8 8.7 %all-to-all-start = ((f32[1,32,192]{2,0,1:T(1,128)}), f32[1,32,192]{2,0,1:T(1,128)S(1)}, u32[]{:S(2)}, u32[]{:S(2)}) async-start(f32[1,32,192]{2,0,1:T(1,128)} %copy.15), calls=%async_computation | async-start | bytes 65536 | tf_op jit(solution)/shard_map/all_to_all | solution.py:26
  40.8 83.6 %copy-start = (bf16[1,768,2048]{2,1,0:T(8,128)(2,1)S(1)}, bf16[1,768,2048]{2,1,0:T(8,128)(2,1)}, u32[]{:S(2)}) copy-start(bf16[1,768,2048]{2,1,0:T(8,128)(2,1)} %all-gather.4.cloned.1.call-done) | copy-start | bytes 9437188
Sparse Core Ops, SparseCore 0:
  9.5 31.2 all-gather.3
  42.9 40.2 all-gather.5
  85.4 38.9 all-gather.7
where the time goes:
time: 137 us
  waiting for transfers between devices  103 us (75%)
  between operations  13.8 us (10%)
  other arithmetic  6.62 us (5%)
  local copies, waits for them, and re-layouts  4.88 us (4%)
  starting transfers between devices  4.38 us (3%)
  matrix products  3.97 us (3%)
    all_gather x1, waiting for transfers between devices, per_device(): lax.all_gather(value_weight, 'sp', axis=0, tiled=True)  41.2 us
    all_gather x1, waiting for transfers between devices, per_device(): lax.all_gather(key_weight, 'sp', axis=0, tiled=True)  39.7 us
    all_gather x1, waiting for transfers between devices, per_device(): piece = lax.all_gather(tokens, 'tp', axis=1, tiled=True)  20.5 us
    all_to_all x1, starting transfers between devices, per_device(): lax.all_to_all(cum_gate, 'tp', split_axis=1, concat_axis=2, tiled=True)  4.26 us
    dot_general x1, matrix products, per_device(): product = jnp.dot(flat, both_weights, preferred_element_type=jnp.float32)  3.45 us
    unnamed x7, local copies, waits for them, and re-layouts  3.08 us
  transfers between devices with their start and end apart: 4, of which 3 were waited for; matrix products, arithmetic and copies ran while one was open for 6% of the time, Pallas kernels for 0%

commit v1 on v0

v1 whole, which is shorter than its diff:
```python
import functools
import math

import jax
import jax.numpy as jnp
from jax import lax
from jax.experimental import pallas as pl
from jax.experimental.pallas import tpu as pltpu
from jax.sharding import PartitionSpec as P

HEAD = 64
CORES = 2
MESH = pl.DeviceIdType.MESH


def row_parts(rows):
    first = max(16, (rows * 13 // 16) // 16 * 16)
    return [(0, first), (first, rows - first)] if first < rows else [(0, rows)]


def kernel(
    sp_size, tp_size, x_size, chunks,
    tok_hbm, gain_ref, wk_hbm, wv_hbm, gate_in, new_gate_ref, query_ref, new_kv_ref,
    kv_hbm, gate_out, read_ref,
    tok, wk, wv, both, scaled, acc, inv, proj, kv_buf, gates,
    in_sem, out_sem, tok_recv, tok_y_send, tok_c_send, w_recv, w_send, g_recv, g_send,
):
    z_size, y_size = sp_size // x_size, tp_size // CORES
    rows, width = wk_hbm.shape
    positions, depth = tok_hbm.shape[1:]
    part = positions // chunks
    parts = row_parts(rows)
    kinds = 2 * len(parts)
    sp, tp = lax.axis_index("sp"), lax.axis_index("tp")
    z, x = sp // x_size, lax.rem(sp, x_size)
    y, core = tp // CORES, lax.rem(tp, CORES)
    other_core = y * CORES + (CORES - 1 - core)

    loads = [
        pltpu.make_async_copy(wk_hbm, wk.at[sp], in_sem.at[0]),
        pltpu.make_async_copy(wv_hbm, wv.at[sp], in_sem.at[1]),
        pltpu.make_async_copy(tok_hbm.at[0], tok.at[tp], in_sem.at[2]),
        pltpu.make_async_copy(gate_in.at[tp], gates.at[tp], in_sem.at[3]),
    ]
    for load in loads:
        load.start()

    x_peers = [lax.rem(x + i, x_size) for i in range(1, x_size)]
    tp_peers = [lax.rem(tp + i, tp_size) for i in range(1, tp_size)]
    above, below = z + 1 < z_size, z >= 1

    barrier = pltpu.get_barrier_semaphore()

    def greet(device):
        pl.semaphore_signal(barrier, inc=1, device_id=device, device_id_type=MESH)

    for peer in tp_peers:
        greet({"sp": sp, "tp": peer})
    for peer in x_peers:
        greet({"sp": z * x_size + peer, "tp": tp})
    pl.when(above)(lambda: greet({"sp": sp + x_size, "tp": tp}))
    pl.when(below)(lambda: greet({"sp": sp - x_size, "tp": tp}))
    pl.semaphore_wait(
        barrier,
        tp_size - 1 + x_size - 1 + above.astype(jnp.int32) + below.astype(jnp.int32),
    )

    sends = []

    def start(copy, cond=None):
        sends.append((copy, cond))
        if cond is None:
            copy.start()
        else:
            pl.when(cond)(copy.start)

    def weight(kind, block):
        first, size = parts[kind // 2]
        return (wk, wv)[kind % 2].at[block, pl.ds(first, size), :]

    def weight_copy(kind, block, way, device_sp):
        return pltpu.make_async_remote_copy(
            src_ref=weight(kind, block),
            dst_ref=weight(kind, block),
            send_sem=w_send.at[kind, block, way],
            recv_sem=w_recv.at[kind, block],
            device_id={"sp": device_sp, "tp": tp},
            device_id_type=MESH,
        )

    def send_up(kind, block, cond):
        start(weight_copy(kind, block, 0, sp + x_size), cond)

    def send_down(kind, block, cond):
        start(weight_copy(kind, block, 1, sp - x_size), cond)

    def send_x(kind, block, cond=None):
        for i, peer in enumerate(x_peers):
            start(weight_copy(kind, block, 2 + i, z * x_size + peer), cond)

    def wait_weight(kind, block, cond=None):
        copy = weight_copy(kind, block, 0, sp)
        if cond is None:
            copy.wait_recv()
        else:
            pl.when(cond)(copy.wait_recv)

    def tok_copy(owner, chunk, send_sem, device_tp):
        piece = tok.at[owner, pl.ds(chunk * part, part), :]
        return pltpu.make_async_remote_copy(
            src_ref=piece,
            dst_ref=piece,
            send_sem=send_sem,
            recv_sem=tok_recv.at[owner, chunk],
            device_id={"sp": sp, "tp": device_tp},
            device_id_type=MESH,
        )

    y_peers = [lax.rem(y + i, y_size) for i in range(1, y_size)]

    loads[0].wait()
    loads[1].wait()
    late_kinds = list(range(2, kinds))
    for kind in late_kinds + [0, 1]:
        send_x(kind, sp)
    for kind in range(kinds):
        send_up(kind, sp, above)
        send_down(kind, sp, below)
    loads[2].wait()
    for chunk in range(chunks):
        for i, peer in enumerate(y_peers):
            start(tok_copy(tp, chunk, tok_y_send.at[i, chunk], peer * CORES + core))
        start(tok_copy(tp, chunk, tok_c_send.at[0, chunk], other_core))
    for i, peer in enumerate(tp_peers):
        start(
            pltpu.make_async_remote_copy(
                src_ref=gate_in.at[peer],
                dst_ref=gates.at[tp],
                send_sem=g_send.at[i],
                recv_sem=g_recv.at[tp],
                device_id={"sp": sp, "tp": peer},
                device_id_type=MESH,
            )
        )

    def scale_rows(owner, first, size):
        piece = tok[owner, pl.ds(first, size), :].astype(jnp.float32)
        square = jnp.mean(piece * piece, axis=-1, keepdims=True)
        inv[owner, pl.ds(first, size), :] = lax.rsqrt(square + 1e-06)
        out = (piece * gain_ref[...]).astype(jnp.bfloat16)
        for s in range(sp_size):
            scaled[s, owner, pl.ds(first, size), :] = out[:, s * rows:(s + 1) * rows]

    def scale_chunk(owner, chunk):
        @pl.loop(0, part // 16)
        def _(i):
            scale_rows(owner, chunk * part + i * 16, 16)

    def pair(block):
        keys, values = wk[block], wv[block]
        pieces = []
        for k in range(width // HEAD):
            pieces += [keys[:, k * HEAD:(k + 1) * HEAD], values[:, k * HEAD:(k + 1) * HEAD]]
        both[block] = jnp.concatenate(pieces, axis=1)

    def add(block, owner):
        acc[owner] += jnp.dot(
            scaled[block, owner], both[block], preferred_element_type=jnp.float32
        )

    def add_near(block):
        pair(block)
        add(block, tp)
        add(block, other_core)

    @pl.loop(0, tp_size)
    def _(i):
        acc[i] = jnp.zeros(acc.shape[1:], jnp.float32)

    for chunk in range(chunks):
        scale_chunk(tp, chunk)
    for chunk in range(chunks):
        tok_copy(other_core, chunk, tok_c_send.at[0, chunk], other_core).wait_recv()
        scale_chunk(other_core, chunk)
    add_near(sp)

    far_owners = [(peer * CORES + core, peer * CORES + (CORES - 1 - core)) for peer in y_peers]

    def pass_tokens(chunk):
        for i, (same, _) in enumerate(far_owners):
            tok_copy(same, chunk, tok_c_send.at[0, chunk], other_core).wait_recv()
            start(tok_copy(same, chunk, tok_c_send.at[1 + i, chunk], other_core))

    def scale_far(chunk):
        for same, cross in far_owners:
            scale_chunk(same, chunk)
            tok_copy(cross, chunk, tok_c_send.at[0, chunk], other_core).wait_recv()
            scale_chunk(cross, chunk)

    reach = jnp.maximum(z, z_size - 1 - z)

    def take_z(d):
        low, high = z - d >= 0, z + d < z_size
        below_block, above_block = sp - d * x_size, sp + d * x_size
        for kind in range(kinds):
            if kind < 2:
                wait_weight(kind, below_block, low)
                send_up(kind, below_block, low & above)
                send_x(kind, below_block, low)
                wait_weight(kind, above_block, high)
                send_down(kind, above_block, high & below)
                send_x(kind, above_block, high)
            else:
                for column in [x] + x_peers:
                    low_block = (z - d) * x_size + column
                    high_block = (z + d) * x_size + column
                    wait_weight(kind, low_block, low)
                    send_up(kind, low_block, low & above)
                    wait_weight(kind, high_block, high)
                    send_down(kind, high_block, high & below)

        @pl.when(low)
        def _():
            add_near(below_block)

        @pl.when(high)
        def _():
            add_near(above_block)

    def take_x(d, now, use):
        for sign in (-1, 1):
            there = (z + sign * d >= 0) & (z + sign * d < z_size) & now
            for column in x_peers:
                block = (z + sign * d) * x_size + column

                @pl.when(there)
                def _(block=block):
                    for kind in range(2):
                        wait_weight(kind, block)
                    use(block)

    steps = max(z_size - 1, 1)
    passed = 0
    for d in range(1, z_size):
        if d == 1:
            for column in x_peers:
                for kind in late_kinds:
                    block = z * x_size + column
                    wait_weight(kind, block)
                    send_up(kind, block, above)
                    send_down(kind, block, below)
            while passed < 1:
                pass_tokens(passed)
                passed += 1
        take_z(d)
        if d == 1:
            for column in x_peers:
                block = z * x_size + column
                for kind in range(2):
                    wait_weight(kind, block)
                add_near(block)
        else:
            take_x(d - 1, d - 1 < reach, add_near)
        while passed < min(chunks - 1, 1 + d * (chunks - 1) // steps):
            pass_tokens(passed)
            passed += 1
    while passed < chunks:
        pass_tokens(passed)
        passed += 1
    for chunk in range(chunks):
        scale_far(chunk)

    @pl.loop(0, sp_size)
    def _(block):
        far = (jnp.abs(block // x_size - z) == reach) & (lax.rem(block, x_size) != x)

        @pl.when(jnp.logical_not(far))
        def _():
            for owners in far_owners:
                for owner in owners:
                    add(block, owner)

    def add_all(block):
        pair(block)

        @pl.loop(0, tp_size)
        def _(owner):
            add(block, owner)

    loads[3].wait()
    for peer in tp_peers:
        pltpu.make_async_remote_copy(
            src_ref=gate_in.at[peer],
            dst_ref=gates.at[peer],
            send_sem=g_send.at[0],
            recv_sem=g_recv.at[peer],
            device_id={"sp": sp, "tp": peer},
            device_id_type=MESH,
        ).wait_recv()
    heads = gate_out.shape[1]
    kv_heads = width // HEAD
    group = heads // kv_heads
    lanes = max(heads, 8)
    gate = jnp.concatenate([gates[i] for i in range(tp_size)], axis=1)
    gate_out[0] = gate
    query = query_ref[...].astype(jnp.float32)
    fresh = new_kv_ref[0].astype(jnp.float32)
    fresh_gate = new_gate_ref[...]

    def padded(list_of_rows, fill):
        missing = lanes - heads
        if missing:
            list_of_rows = list_of_rows + [jnp.full((missing, fill), 0.0, jnp.float32)]
        return jnp.concatenate(list_of_rows, axis=0)

    query_rows = padded([query[:, h * HEAD:(h + 1) * HEAD] for h in range(heads)], HEAD)
    fresh_rows = padded([fresh[h // group:h // group + 1, :] for h in range(heads)], 2 * HEAD)
    scale_factor = 1.0 / math.sqrt(HEAD)
    own = jnp.sum(query_rows * fresh_rows[:, :HEAD], axis=1, keepdims=True) * scale_factor
    own_value = fresh_rows[:, HEAD:]
    pick = lax.broadcasted_iota(jnp.int32, (lanes, heads), 0) == lax.broadcasted_iota(
        jnp.int32, (lanes, heads), 1
    )
    gate_column = jnp.sum(jnp.where(pick, fresh_gate, 0.0), axis=1, keepdims=True)
    if lanes > heads:
        gate = jnp.concatenate(
            [gate, jnp.zeros((lanes - heads, gate.shape[1]), jnp.float32)], axis=0
        )
    bias = gate_column - gate
    head_of = lax.broadcasted_iota(jnp.int32, (lanes, 2 * HEAD), 0) // group
    wide = jnp.concatenate([query_rows, jnp.zeros_like(query_rows)], axis=1)
    wide = jnp.concatenate(
        [jnp.where(head_of == k, wide, 0.0) for k in range(kv_heads)], axis=1
    ).astype(jnp.bfloat16)

    for d in range(z_size):
        take_x(d, reach == d, add_all) if d else None

    for owner in range(tp_size):
        out = (acc[owner] * inv[owner]).astype(jnp.bfloat16)
        proj[pl.ds(owner * positions, positions), :] = out
        for k in range(kv_heads):
            kv_buf[0, k, pl.ds(owner * positions, positions), :] = out[
                :, 2 * k * HEAD:2 * (k + 1) * HEAD
            ]
    store = pltpu.make_async_copy(kv_buf, kv_hbm, out_sem)
    store.start()

    score = lax.dot_general(
        wide, proj[...], (((1,), (1,)), ((), ())), preferred_element_type=jnp.float32
    )
    score = score * scale_factor + bias
    top = jnp.maximum(jnp.max(score, axis=1, keepdims=True), own)
    expo = jnp.exp(score - top)
    own_factor = jnp.exp(own - top)
    total = jnp.sum(expo, axis=1, keepdims=True) + own_factor
    read = jnp.dot(expo.astype(jnp.bfloat16), proj[...], preferred_element_type=jnp.float32)
    value_of = lax.broadcasted_iota(jnp.int32, (lanes, HEAD), 0) // group
    numer = own_factor * own_value
    for k in range(kv_heads):
        numer += jnp.where(value_of == k, read[:, (2 * k + 1) * HEAD:(2 * k + 2) * HEAD], 0.0)
    result = numer / total
    read_ref[...] = jnp.concatenate(
        [result[h:h + 1, :] for h in range(heads)], axis=1
    ).astype(jnp.bfloat16)

    for copy, cond in sends:
        if cond is None:
            copy.wait_send()
        else:
            pl.when(cond)(copy.wait_send)
    store.wait()


def per_device(sp_size, tp_size, tokens, norm_gain, key_weight, value_weight, cum_gate, new_gate, new_query, new_kv):
    _, positions, depth = tokens.shape
    rows, width = key_weight.shape
    heads_all = cum_gate.shape[1]
    heads = heads_all // tp_size
    kv_heads = width // HEAD
    length = positions * tp_size
    x_size = 1 << (int(math.log2(sp_size)) // 2)
    chunks = 4
    kinds = 2 * len(row_parts(rows))
    y_size = tp_size // CORES
    any_spec = pl.BlockSpec(memory_space=pl.ANY)
    vmem = pl.BlockSpec(memory_space=pltpu.VMEM)
    dma = pltpu.SemaphoreType.DMA
    return pl.pallas_call(
        functools.partial(kernel, sp_size, tp_size, x_size, chunks),
        out_shape=(
            jax.ShapeDtypeStruct((1, kv_heads, length, 2 * HEAD), jnp.bfloat16),
            jax.ShapeDtypeStruct((1, heads, length), jnp.float32),
            jax.ShapeDtypeStruct((1, heads * HEAD), jnp.bfloat16),
        ),
        in_specs=[any_spec, vmem, any_spec, any_spec, vmem, vmem, vmem, vmem],
        out_specs=(any_spec, vmem, vmem),
        scratch_shapes=[
            pltpu.VMEM((tp_size, positions, depth), jnp.bfloat16),
            pltpu.VMEM((sp_size, rows, width), jnp.bfloat16),
            pltpu.VMEM((sp_size, rows, width), jnp.bfloat16),
            pltpu.VMEM((sp_size, rows, 2 * width), jnp.bfloat16),
            pltpu.VMEM((sp_size, tp_size, positions, rows), jnp.bfloat16),
            pltpu.VMEM((tp_size, positions, 2 * width), jnp.float32),
            pltpu.VMEM((tp_size, positions, 1), jnp.float32),
            pltpu.VMEM((length, 2 * width), jnp.bfloat16),
            pltpu.VMEM((1, kv_heads, length, 2 * HEAD), jnp.bfloat16),
            pltpu.VMEM((tp_size, heads, positions), jnp.float32),
            dma((4,)),
            dma,
            dma((tp_size, chunks)),
            dma((max(y_size - 1, 1), chunks)),
            dma((y_size, chunks)),
            dma((kinds, sp_size)),
            dma((kinds, sp_size, 1 + x_size)),
            dma((tp_size,)),
            dma((tp_size,)),
        ],
        compiler_params=pltpu.CompilerParams(
            collective_id=0, has_side_effects=True, vmem_limit_bytes=62 * 1024 * 1024
        ),
        name="prefill",
    )(
        tokens, norm_gain.reshape(1, depth), key_weight, value_weight,
        cum_gate.reshape(tp_size, heads, positions), new_gate, new_query, new_kv,
    )


def solution(mesh):
    in_specs = (
        P("sp", "tp", None),
        P(),
        P("sp", "tp"),
        P("sp", "tp"),
        P("sp", None, "tp"),
        P("sp", "tp"),
        P("sp", "tp"),
        P("sp", "tp", None),
    )
    out_specs = (P("sp", "tp", None, None), P("sp", "tp", None), P("sp", "tp"))
    return jax.shard_map(
        functools.partial(per_device, mesh.shape["sp"], mesh.shape["tp"]),
        mesh=mesh, in_specs=in_specs, out_specs=out_specs, check_vma=False,
    )
```

time: 137 us -> 40.4 us (0.29)
  waiting for transfers between devices: 103 us -> 0 us
  Pallas kernels: 0 us -> 36.2 us
  between operations: 13.8 us -> 0.65 us
  other arithmetic: 6.62 us -> 0 us
  starting transfers between devices: 4.38 us -> 0 us
  matrix products: 3.97 us -> 0 us
  local copies, waits for them, and re-layouts: 4.88 us -> 3.32 us
    all_gather x3 -> x0, waiting for transfers between devices: 101 us -> none  [the longest x1 41.2 us: per_device(): lax.all_gather(value_weight, 'sp', axis=0, tiled=True)]
    pallas_call x0 -> x1, Pallas kernels: none -> 36.2 us  [per_device(): pl.pallas_call(functools.partial(kernel, sp_size, tp_size, x_size, chunks...]
    all_to_all x1 -> x0, starting transfers between devices: 4.26 us -> none  [per_device(): lax.all_to_all(cum_gate, 'tp', split_axis=1, concat_axis=2, tiled=True)]
    dot_general x3 -> x0, matrix products: 3.97 us -> none  [the longest x1 3.45 us: per_device(): product = jnp.dot(flat, both_weights, preferred_element_type=jnp.float32)]
    reduce_sum x3 -> x0, other arithmetic: 2.99 us -> none  [the longest x1 2.72 us: normalize(): jnp.mean(widened * widened, axis=-1, keepdims=True) + 1e-06]
    unnamed x3 -> x0, waiting for transfers between devices: 2.06 us -> none
    unnamed x2 -> x0, other arithmetic: 2.03 us -> none
  transfers between devices with their start and end apart: 4 -> 0, of which waited for: 3 -> 0; matrix products, arithmetic and copies ran while one was open for 6% -> 0% of each run, Pallas kernels for 0% -> 0%
where the time goes in v1:
time: 40.4 us; the launch traced here: 40.2 us
  Pallas kernels  36.2 us (90%)
  local copies, waits for them, and re-layouts  3.32 us (8%)
  between operations  0.65 us (2%)
    pallas_call x1, Pallas kernels, per_device(): pl.pallas_call(functools.partial(kernel, sp_size, tp_size, x_size, chunks...  36.2 us
    unnamed x7, local copies, waits for them, and re-layouts  3.32 us

profile of v1, /device:TPU:0, one launch (start us, length us, event | category | flops | bytes accessed | tf_op | source)
XLA Modules:
  0.0 40.2 jit_solution(303037239773909061)
XLA Ops:
  0.6 36.2 %prefill.1 = (bf16[1,4,768,128]{3,2,1,0:T(8,128)(2,1)}, f32[1,8,768]{2,1,0:T(8,128)}, bf16[1,512]{1,0:T(2,128)(2,1)}) custom-call(bf16[1,192,2048]{2,1,0:T(8,128)(2,1)} %tok_hbm.1, f32[1,2048]{1,0:T(1,128)} %bitcast.3, bf16[256,256]{1,0:T(8,128)(2,1)} %wk_hbm.1, bf16[256,256]{1,0:T(8,128)(2,1)} %wv_hbm.1, f32[4,8,192]{2,1,0:T(8,128)} %bitcast.2, ...), custom_call_target="tpu_custom_call" | custom-call | tf_op jit(solution)/shard_map/prefill/pallas_call | solution.py:389
  36.8 0.0 copy-start
  36.8 2.1 %copy.14 = bf16[1,4,768,128]{3,2,1,0:T(8,128)(2,1)} copy(bf16[1,4,768,128]{3,2,1,0:T(8,128)(2,1)} %get-tuple-element.6) | data formatting | bytes 1572864
  38.9 0.0 copy-done
  38.9 0.0 copy-start.1
  38.9 0.6 %copy.15 = f32[1,8,768]{2,1,0:T(8,128)} copy(f32[1,8,768]{2,1,0:T(8,128)S(1)} %copy-done) | data formatting | bytes 49152
  39.5 0.1 copy-done.1
  39.6 0.6 %copy.16 = bf16[1,512]{1,0:T(2,128)(2,1)} copy(bf16[1,512]{1,0:T(2,128)(2,1)S(1)} %copy-done.1) | data formatting | bytes 2048
Async XLA Ops:
  36.8 2.1 %copy-start = (f32[1,8,768]{2,1,0:T(8,128)S(1)}, f32[1,8,768]{2,1,0:T(8,128)}, u32[]{:S(2)}) copy-start(f32[1,8,768]{2,1,0:T(8,128)} %get-tuple-element.7) | copy-start | bytes 73732
  38.9 0.7 %copy-start.1 = (bf16[1,512]{1,0:T(2,128)(2,1)S(1)}, bf16[1,512]{1,0:T(2,128)(2,1)}, u32[]{:S(2)}) copy-start(bf16[1,512]{1,0:T(2,128)(2,1)} %get-tuple-element.8) | copy-start | bytes 3076

commit v2 on v1

v2 whole, which is shorter than its diff:
```python
import functools
import math

import jax
import jax.numpy as jnp
from jax import lax
from jax.experimental import pallas as pl
from jax.experimental.pallas import tpu as pltpu
from jax.sharding import PartitionSpec as P

HEAD = 64
CORES = 2
MESH = pl.DeviceIdType.MESH


def kernel(
    sp_size, tp_size, x_size, chunks,
    tok_hbm, gain_hbm, wk_hbm, wv_hbm, gate_hbm, new_gate_hbm, query_hbm, new_kv_hbm,
    kv_out, gate_out, bias_out, wide_out, own_out, own_value_out,
    gain_ref, gate_in, new_gate_ref, query_ref, new_kv_ref, tok, wk, wv, both, scaled, acc, inv, gates,
    in_sem, tok_recv, tok_y_send, tok_c_send, w_recv, w_send, g_recv, g_send,
):
    z_size, y_size = sp_size // x_size, tp_size // CORES
    rows, width = wk_hbm.shape
    positions, depth = tok_hbm.shape[1:]
    part = positions // chunks
    sp, tp = lax.axis_index("sp"), lax.axis_index("tp")
    z, x = sp // x_size, lax.rem(sp, x_size)
    y, core = tp // CORES, lax.rem(tp, CORES)
    other_core = y * CORES + (CORES - 1 - core)

    loads = [
        pltpu.make_async_copy(wk_hbm, wk.at[sp], in_sem.at[0]),
        pltpu.make_async_copy(wv_hbm, wv.at[sp], in_sem.at[1]),
        pltpu.make_async_copy(tok_hbm.at[0], tok.at[tp], in_sem.at[2]),
        pltpu.make_async_copy(gate_hbm, gate_in, in_sem.at[3]),
        pltpu.make_async_copy(gain_hbm, gain_ref, in_sem.at[4]),
        pltpu.make_async_copy(new_gate_hbm, new_gate_ref, in_sem.at[5]),
        pltpu.make_async_copy(query_hbm, query_ref, in_sem.at[6]),
        pltpu.make_async_copy(new_kv_hbm, new_kv_ref, in_sem.at[7]),
    ]
    for load in loads:
        load.start()

    x_peers = [lax.rem(x + i, x_size) for i in range(1, x_size)]
    tp_peers = [lax.rem(tp + i, tp_size) for i in range(1, tp_size)]
    above, below = z + 1 < z_size, z >= 1

    barrier = pltpu.get_barrier_semaphore()

    def greet(device):
        pl.semaphore_signal(barrier, inc=1, device_id=device, device_id_type=MESH)

    for peer in tp_peers:
        greet({"sp": sp, "tp": peer})
    for peer in x_peers:
        greet({"sp": z * x_size + peer, "tp": tp})
    pl.when(above)(lambda: greet({"sp": sp + x_size, "tp": tp}))
    pl.when(below)(lambda: greet({"sp": sp - x_size, "tp": tp}))
    pl.semaphore_wait(
        barrier,
        tp_size - 1 + x_size - 1 + above.astype(jnp.int32) + below.astype(jnp.int32),
    )

    sends = []

    def start(copy, cond=None):
        sends.append((copy, cond))
        if cond is None:
            copy.start()
        else:
            pl.when(cond)(copy.start)

    def weight(kind, block):
        return (wk, wv)[kind].at[block]

    def weight_copy(kind, block, way, device_sp):
        return pltpu.make_async_remote_copy(
            src_ref=weight(kind, block),
            dst_ref=weight(kind, block),
            send_sem=w_send.at[kind, block, way],
            recv_sem=w_recv.at[kind, block],
            device_id={"sp": device_sp, "tp": tp},
            device_id_type=MESH,
        )

    def send_up(kind, block, cond):
        start(weight_copy(kind, block, 0, sp + x_size), cond)

    def send_down(kind, block, cond):
        start(weight_copy(kind, block, 1, sp - x_size), cond)

    def send_x(kind, block, cond=None):
        for i, peer in enumerate(x_peers):
            start(weight_copy(kind, block, 2 + i, z * x_size + peer), cond)

    def wait_weight(kind, block, cond=None):
        copy = weight_copy(kind, block, 0, sp)
        if cond is None:
            copy.wait_recv()
        else:
            pl.when(cond)(copy.wait_recv)

    def tok_copy(owner, chunk, send_sem, device_tp):
        piece = tok.at[owner, pl.ds(chunk * part, part), :]
        return pltpu.make_async_remote_copy(
            src_ref=piece,
            dst_ref=piece,
            send_sem=send_sem,
            recv_sem=tok_recv.at[owner, chunk],
            device_id={"sp": sp, "tp": device_tp},
            device_id_type=MESH,
        )

    y_peers = [lax.rem(y + i, y_size) for i in range(1, y_size)]

    loads[0].wait()
    loads[1].wait()
    for kind in (1, 0):
        send_x(kind, sp)
    for kind in range(2):
        send_up(kind, sp, above)
        send_down(kind, sp, below)
    loads[2].wait()
    for chunk in range(chunks):
        for i, peer in enumerate(y_peers):
            start(tok_copy(tp, chunk, tok_y_send.at[i, chunk], peer * CORES + core))
        start(tok_copy(tp, chunk, tok_c_send.at[0, chunk], other_core))
    loads[3].wait()
    for i, peer in enumerate(tp_peers):
        start(
            pltpu.make_async_remote_copy(
                src_ref=gate_in.at[peer],
                dst_ref=gates.at[tp],
                send_sem=g_send.at[i],
                recv_sem=g_recv.at[tp],
                device_id={"sp": sp, "tp": peer},
                device_id_type=MESH,
            )
        )

    def scale_rows(owner, first, size):
        piece = tok[owner, pl.ds(first, size), :].astype(jnp.float32)
        square = jnp.mean(piece * piece, axis=-1, keepdims=True)
        inv[owner, pl.ds(first, size), :] = lax.rsqrt(square + 1e-06)
        out = (piece * gain_ref[...]).astype(jnp.bfloat16)
        for s in range(sp_size):
            scaled[s, owner, pl.ds(first, size), :] = out[:, s * rows:(s + 1) * rows]

    def scale_chunk(owner, chunk):
        @pl.loop(0, part // 16)
        def _(i):
            scale_rows(owner, chunk * part + i * 16, 16)

    def pair(block):
        keys, values = wk[block], wv[block]
        pieces = []
        for k in range(width // HEAD):
            pieces += [keys[:, k * HEAD:(k + 1) * HEAD], values[:, k * HEAD:(k + 1) * HEAD]]
        both[block] = jnp.concatenate(pieces, axis=1)

    def add(block, owner):
        acc[owner] += jnp.dot(
            scaled[block, owner], both[block], preferred_element_type=jnp.float32
        )

    def add_near(block):
        pair(block)
        add(block, tp)
        add(block, other_core)

    @pl.loop(0, tp_size)
    def _(i):
        acc[i] = jnp.zeros(acc.shape[1:], jnp.float32)

    loads[4].wait()
    for chunk in range(chunks):
        scale_chunk(tp, chunk)
    for chunk in range(chunks):
        tok_copy(other_core, chunk, tok_c_send.at[0, chunk], other_core).wait_recv()
        scale_chunk(other_core, chunk)
    add_near(sp)

    far_owners = [(peer * CORES + core, peer * CORES + (CORES - 1 - core)) for peer in y_peers]

    def pass_tokens(chunk):
        for i, (same, _) in enumerate(far_owners):
            tok_copy(same, chunk, tok_c_send.at[0, chunk], other_core).wait_recv()
            start(tok_copy(same, chunk, tok_c_send.at[1 + i, chunk], other_core))

    def scale_far(chunk):
        for same, cross in far_owners:
            scale_chunk(same, chunk)
            tok_copy(cross, chunk, tok_c_send.at[0, chunk], other_core).wait_recv()
            scale_chunk(cross, chunk)

    reach = jnp.maximum(z, z_size - 1 - z)

    def sides(d):
        return (sp - d * x_size, z - d >= 0), (sp + d * x_size, z + d < z_size)

    def ends(d):
        if z_size < 3:
            return False, False
        return z - d == 0, z + d == z_size - 1

    def no(flag):
        return True if flag is False else jnp.logical_not(flag)

    def take_first(d):
        (low_block, low), (high_block, high) = sides(d)
        low_end, high_end = ends(d)
        for kind in range(2):
            wait_weight(kind, low_block, low)
            send_up(kind, low_block, low & above)
            send_x(kind, low_block, low & no(low_end) if kind else low)
            wait_weight(kind, high_block, high)
            send_down(kind, high_block, high & below)
            send_x(kind, high_block, high & no(high_end) if kind else high)

    def take_late(d):
        if z_size < 3:
            return
        (low_block, _), (high_block, _) = sides(d)
        low_end, high_end = ends(d)
        for column in x_peers:
            wait_weight(1, low_block - x + column, low_end)
            send_up(1, low_block - x + column, low_end & above)
            wait_weight(1, high_block - x + column, high_end)
            send_down(1, high_block - x + column, high_end & below)

    def take_x(d, now, use):
        for (block, there), end in zip(sides(d), ends(d)):
            for column in x_peers:

                @pl.when(there & now)
                def _(block=block - x + column, end=end):
                    wait_weight(0, block)
                    if end is False:
                        wait_weight(1, block)
                    else:
                        pl.when(jnp.logical_not(end))(lambda: wait_weight(1, block))
                    use(block)

    passed = 0

    def pass_up_to(limit):
        nonlocal passed
        while passed < limit:
            pass_tokens(passed)
            if passed:
                scale_far(passed - 1)
            passed += 1

    for column in x_peers:
        block = z * x_size + column
        wait_weight(1, block)
        if z_size > 2:
            send_up(1, block, z == 0)
            send_down(1, block, z == z_size - 1)
    steps = max(z_size - 1, 1)
    for d in range(1, z_size):
        take_first(d)
        if d == 1:
            pass_up_to(1)
            for column in x_peers:
                wait_weight(0, z * x_size + column)
                add_near(z * x_size + column)
        for block, there in sides(d):

            @pl.when(there)
            def _(block=block):
                add_near(block)

        if d > 1:
            take_x(d - 1, d - 1 < reach, add_near)
        if d < z_size - 1:
            take_late(d)
        pass_up_to(min(chunks - 1, d * (chunks - 1) // steps))
    pass_up_to(chunks)
    scale_far(chunks - 1)

    @pl.loop(0, sp_size)
    def _(block):
        last = (jnp.abs(block // x_size - z) == reach) & (lax.rem(block, x_size) != x)

        @pl.when(jnp.logical_not(last))
        def _():
            for owners in far_owners:
                for owner in owners:
                    add(block, owner)

    def add_all(block):
        pair(block)

        @pl.loop(0, tp_size)
        def _(owner):
            add(block, owner)

    for peer in tp_peers:
        pltpu.make_async_remote_copy(
            src_ref=gate_in.at[peer],
            dst_ref=gates.at[peer],
            send_sem=g_send.at[0],
            recv_sem=g_recv.at[peer],
            device_id={"sp": sp, "tp": peer},
            device_id_type=MESH,
        ).wait_recv()
    kv_heads = width // HEAD
    gates[tp] = gate_in[tp]
    gate = jnp.concatenate([gates[i] for i in range(tp_size)], axis=1)
    gate_out[...] = gate
    for load in loads[5:]:
        load.wait()
    heads = gate_out.shape[0]
    group = heads // kv_heads
    lanes = max(heads, 8)
    query = query_ref[...].astype(jnp.float32)
    fresh = new_kv_ref[0].astype(jnp.float32)
    fresh_gate = new_gate_ref[...]

    def padded(list_of_rows, fill):
        missing = lanes - heads
        if missing:
            list_of_rows = list_of_rows + [jnp.full((missing, fill), 0.0, jnp.float32)]
        return jnp.concatenate(list_of_rows, axis=0)

    query_rows = padded([query[:, h * HEAD:(h + 1) * HEAD] for h in range(heads)], HEAD)
    fresh_rows = padded([fresh[h // group:h // group + 1, :] for h in range(heads)], 2 * HEAD)
    scale_factor = 1.0 / math.sqrt(HEAD)
    own = jnp.sum(query_rows * fresh_rows[:, :HEAD], axis=1, keepdims=True) * scale_factor
    own_value = fresh_rows[:, HEAD:]
    pick = lax.broadcasted_iota(jnp.int32, (lanes, heads), 0) == lax.broadcasted_iota(
        jnp.int32, (lanes, heads), 1
    )
    gate_column = jnp.sum(jnp.where(pick, fresh_gate, 0.0), axis=1, keepdims=True)
    if lanes > heads:
        gate = jnp.concatenate(
            [gate, jnp.zeros((lanes - heads, gate.shape[1]), jnp.float32)], axis=0
        )
    bias = gate_column - gate
    head_of = lax.broadcasted_iota(jnp.int32, (lanes, 2 * HEAD), 0) // group
    wide = jnp.concatenate([query_rows, jnp.zeros_like(query_rows)], axis=1)
    bias_out[...] = bias
    for k in range(kv_heads):
        wide_out[k] = jnp.where(head_of == k, wide, 0.0).astype(jnp.bfloat16)
    own_out[...] = jnp.broadcast_to(own, own_out.shape)
    own_value_out[...] = own_value

    if z_size > 1:
        take_late(z_size - 1)
    for d in range(1, z_size):
        take_x(d, reach == d, add_all)

    for owner in range(tp_size):
        out = (acc[owner] * inv[owner]).astype(jnp.bfloat16)
        for k in range(kv_heads):
            kv_out[k, pl.ds(owner * positions, positions), :] = out[
                :, 2 * k * HEAD:2 * (k + 1) * HEAD
            ]

    for copy, cond in sends:
        if cond is None:
            copy.wait_send()
        else:
            pl.when(cond)(copy.wait_send)


def read_kernel(kv, gate, bias_ref, wide, own_ref, own_value_ref, kv_hbm, gate_hbm, read_ref, sem):
    stores = [
        pltpu.make_async_copy(kv, kv_hbm.at[0], sem.at[0]),
        pltpu.make_async_copy(gate, gate_hbm.at[0], sem.at[1]),
    ]
    for store in stores:
        store.start()
    heads = gate.shape[0]
    kv_heads, lanes = wide.shape[:2]
    group = heads // kv_heads
    own, bias, own_value = own_ref[:, :1], bias_ref[...], own_value_ref[...]
    score = 0.0
    for k in range(kv_heads):
        score += lax.dot_general(
            wide[k], kv[k], (((1,), (1,)), ((), ())), preferred_element_type=jnp.float32
        )
    score = score * (1.0 / math.sqrt(HEAD)) + bias
    top = jnp.maximum(jnp.max(score, axis=1, keepdims=True), own)
    expo = jnp.exp(score - top)
    own_factor = jnp.exp(own - top)
    total = jnp.sum(expo, axis=1, keepdims=True) + own_factor
    weights = expo.astype(jnp.bfloat16)
    value_of = lax.broadcasted_iota(jnp.int32, (lanes, HEAD), 0) // group
    numer = own_factor * own_value
    for k in range(kv_heads):
        read = jnp.dot(weights, kv[k], preferred_element_type=jnp.float32)
        numer += jnp.where(value_of == k, read[:, HEAD:], 0.0)
    result = numer / total
    read_ref[...] = jnp.concatenate(
        [result[h:h + 1, :] for h in range(heads)], axis=1
    ).astype(jnp.bfloat16)
    for store in stores:
        store.wait()


def per_device(sp_size, tp_size, tokens, norm_gain, key_weight, value_weight, cum_gate, new_gate, new_query, new_kv):
    _, positions, depth = tokens.shape
    rows, width = key_weight.shape
    heads_all = cum_gate.shape[1]
    heads = heads_all // tp_size
    kv_heads = width // HEAD
    length = positions * tp_size
    x_size = 1 << (int(math.log2(sp_size)) // 2)
    chunks = 4
    y_size = tp_size // CORES
    any_spec = pl.BlockSpec(memory_space=pl.ANY)
    vmem = pl.BlockSpec(memory_space=pltpu.VMEM)
    dma = pltpu.SemaphoreType.DMA
    bf16, f32 = jnp.bfloat16, jnp.float32
    lanes = max(heads, 8)
    buffers = [
        ((1, depth), f32),
        ((tp_size, heads, positions), f32),
        ((1, heads), f32),
        ((1, heads * HEAD), bf16),
        ((1, kv_heads, 2 * HEAD), bf16),
        ((tp_size, positions, depth), bf16),
        ((sp_size, rows, width), bf16),
        ((sp_size, rows, width), bf16),
        ((sp_size, rows, 2 * width), bf16),
        ((sp_size, tp_size, positions, rows), bf16),
        ((tp_size, positions, 2 * width), f32),
        ((tp_size, positions, 1), f32),
        ((tp_size, heads, positions), f32),
    ]
    need = sum(
        math.prod(shape[:-1]) * -(-shape[-1] // 128) * 128 * jnp.dtype(kind).itemsize
        for shape, kind in buffers
    )
    results = pl.pallas_call(
        functools.partial(kernel, sp_size, tp_size, x_size, chunks),
        out_shape=(
            jax.ShapeDtypeStruct((kv_heads, length, 2 * HEAD), bf16),
            jax.ShapeDtypeStruct((heads, length), f32),
            jax.ShapeDtypeStruct((lanes, length), f32),
            jax.ShapeDtypeStruct((kv_heads, lanes, 2 * HEAD), bf16),
            jax.ShapeDtypeStruct((lanes, 2 * HEAD), f32),
            jax.ShapeDtypeStruct((lanes, HEAD), f32),
        ),
        in_specs=[pl.BlockSpec(memory_space=pltpu.HBM)] * 8,
        out_specs=(vmem,) * 6,
        scratch_shapes=[pltpu.VMEM(shape, kind) for shape, kind in buffers] + [
            dma((8,)),
            dma((tp_size, chunks)),
            dma((max(y_size - 1, 1), chunks)),
            dma((y_size, chunks)),
            dma((2, sp_size)),
            dma((2, sp_size, 1 + x_size)),
            dma((tp_size,)),
            dma((tp_size,)),
        ],
        compiler_params=pltpu.CompilerParams(
            collective_id=0, has_side_effects=True,
            vmem_limit_bytes=min(62 * 1024 * 1024, need + 6 * 1024 * 1024),
        ),
        name="prefill",
    )(
        *(
            pltpu.with_memory_space_constraint(array, pltpu.HBM)
            for array in (
                tokens, norm_gain.reshape(1, depth), key_weight, value_weight,
                cum_gate.reshape(tp_size, heads, positions), new_gate, new_query, new_kv,
            )
        )
    )
    return pl.pallas_call(
        read_kernel,
        out_shape=(
            jax.ShapeDtypeStruct((1, kv_heads, length, 2 * HEAD), bf16),
            jax.ShapeDtypeStruct((1, heads, length), f32),
            jax.ShapeDtypeStruct((1, heads * HEAD), bf16),
        ),
        in_specs=[vmem] * 6,
        out_specs=(any_spec, any_spec, vmem),
        scratch_shapes=[dma((2,))],
        compiler_params=pltpu.CompilerParams(vmem_limit_bytes=8 * 1024 * 1024),
        name="first_read",
    )(*results)


def solution(mesh):
    in_specs = (
        P("sp", "tp", None),
        P(),
        P("sp", "tp"),
        P("sp", "tp"),
        P("sp", None, "tp"),
        P("sp", "tp"),
        P("sp", "tp"),
        P("sp", "tp", None),
    )
    out_specs = (P("sp", "tp", None, None), P("sp", "tp", None), P("sp", "tp"))
    return jax.shard_map(
        functools.partial(per_device, mesh.shape["sp"], mesh.shape["tp"]),
        mesh=mesh, in_specs=in_specs, out_specs=out_specs, check_vma=False,
    )
```

time: 40.4 us -> 32.9 us (0.81)
  Pallas kernels: 36.2 us -> 32.1 us
  local copies, waits for them, and re-layouts: 3.32 us -> 0 us
    pallas_call x1, Pallas kernels: 36.2 us -> 30.5 us  [per_device(): pl.pallas_call(functools.partial(kernel, sp_size, tp_size, x_size, chunks...]
    unnamed x7 -> x0, local copies, waits for them, and re-layouts: 3.32 us -> none
    pallas_call x0 -> x1, Pallas kernels: none -> 1.57 us  [per_device(): pl.pallas_call(read_kernel, out_shape=(jax.ShapeDtypeStruct((1, kv_heads,...]
where the time goes in v2:
time: 32.9 us; the launch traced here: 32.8 us
  Pallas kernels  32.1 us (98%)
  between operations  0.64 us (2%)
    pallas_call x1, Pallas kernels, per_device(): pl.pallas_call(functools.partial(kernel, sp_size, tp_size, x_size, chunks...  30.5 us
    pallas_call x1, Pallas kernels, per_device(): pl.pallas_call(read_kernel, out_shape=(jax.ShapeDtypeStruct((1, kv_heads,...  1.57 us

profile of v2, /device:TPU:0, one launch (start us, length us, event | category | flops | bytes accessed | tf_op | source)
XLA Modules:
  0.0 32.8 jit_solution(16214282497455396872)
XLA Ops:
  0.6 30.5 %prefill.1 = (bf16[4,768,128]{2,1,0:T(8,128)(2,1)S(1)}, f32[8,768]{1,0:T(8,128)S(1)}, f32[8,768]{1,0:T(8,128)S(1)}, bf16[4,8,128]{2,1,0:T(8,128)(2,1)S(1)}, f32[8,128]{1,0:T(8,128)S(1)}, /*index=5*/f32[8,64]{1,0:T(8,128)S(1)}) custom-call(bf16[1,192,2048]{2,1,0:T(8,128)(2,1)} %tok_hbm.1, f32[1,2048]{1,0:T(1,128)} %bitcast.3, bf16[256,256]{1,0:T(8,128)(2,1)} %wk_hbm.1, ...), custom_call_target="tpu_custom_call" | custom-call | tf_op jit(solution)/shard_map/prefill/pallas_call | solution.py:438
  31.2 1.6 %first_read.1 = (bf16[1,4,768,128]{3,2,1,0:T(8,128)(2,1)}, f32[1,8,768]{2,1,0:T(8,128)}, bf16[1,512]{1,0:T(2,128)(2,1)}) custom-call(bf16[4,768,128]{2,1,0:T(8,128)(2,1)S(1)} %get-tuple-element.9.kv, f32[8,768]{1,0:T(8,128)S(1)} %get-tuple-element.10.gate, f32[8,768]{1,0:T(8,128)S(1)} %get-tuple-element.11.bias_ref, ...), custom_call_target="tpu_custom_call" | custom-call | tf_op jit(solution)/shard_map/first_read/pallas_call | solution.py:474

commit v3 on v2

--- a/solution.py
+++ b/solution.py
@@ -409,7 +409,7 @@
     kv_heads = width // HEAD
     length = positions * tp_size
     x_size = 1 << (int(math.log2(sp_size)) // 2)
-    chunks = 4
+    chunks = 6
     y_size = tp_size // CORES
     any_spec = pl.BlockSpec(memory_space=pl.ANY)
     vmem = pl.BlockSpec(memory_space=pltpu.VMEM)

time: 32.9 us -> 33.4 us (1.015)
  Pallas kernels: 32.1 us -> 32.6 us
    pallas_call x1, Pallas kernels: 30.5 us -> 31.1 us  [per_device(): pl.pallas_call(functools.partial(kernel, sp_size, tp_size, x_size, chunks...]
where the time goes in v3:
time: 33.4 us; the launch traced here: 33.3 us
  Pallas kernels  32.6 us (98%)
  between operations  0.64 us (2%)
    pallas_call x1, Pallas kernels, per_device(): pl.pallas_call(functools.partial(kernel, sp_size, tp_size, x_size, chunks...  31.1 us
    pallas_call x1, Pallas kernels, per_device(): pl.pallas_call(read_kernel, out_shape=(jax.ShapeDtypeStruct((1, kv_heads,...  1.57 us

profile of v3, /device:TPU:0, one launch (start us, length us, event | category | flops | bytes accessed | tf_op | source)
XLA Modules:
  0.0 33.3 jit_solution(12499421739344781170)
XLA Ops:
  0.6 31.1 %prefill.1 = (bf16[4,768,128]{2,1,0:T(8,128)(2,1)S(1)}, f32[8,768]{1,0:T(8,128)S(1)}, f32[8,768]{1,0:T(8,128)S(1)}, bf16[4,8,128]{2,1,0:T(8,128)(2,1)S(1)}, f32[8,128]{1,0:T(8,128)S(1)}, /*index=5*/f32[8,64]{1,0:T(8,128)S(1)}) custom-call(bf16[1,192,2048]{2,1,0:T(8,128)(2,1)} %tok_hbm.1, f32[1,2048]{1,0:T(1,128)} %bitcast.3, bf16[256,256]{1,0:T(8,128)(2,1)} %wk_hbm.1, ...), custom_call_target="tpu_custom_call" | custom-call | tf_op jit(solution)/shard_map/prefill/pallas_call | solution.py:438
  31.7 1.6 %first_read.1 = (bf16[1,4,768,128]{3,2,1,0:T(8,128)(2,1)}, f32[1,8,768]{2,1,0:T(8,128)}, bf16[1,512]{1,0:T(2,128)(2,1)}) custom-call(bf16[4,768,128]{2,1,0:T(8,128)(2,1)S(1)} %get-tuple-element.9.kv, f32[8,768]{1,0:T(8,128)S(1)} %get-tuple-element.10.gate, f32[8,768]{1,0:T(8,128)S(1)} %get-tuple-element.11.bias_ref, ...), custom_call_target="tpu_custom_call" | custom-call | tf_op jit(solution)/shard_map/first_read/pallas_call | solution.py:474
